TPU v7x, 256 devices: a whole 4x4x8 slice. The times are simulated.
256 devices in a mesh: sp: 16 (over y, x), tp: 16 (over z, core).
Axes of the slice: x: 4, y: 4, z: 8, core: 2. Of those that a mesh axis runs over, the one named last changes fastest.
Arguments:
- queries: bfloat16 [32768, 2048], P('sp', 'tp'), may hold values from -160 to 160
- key_heads: bfloat16 [32768, 512], P('sp'), may hold values from -8 to 8
- value_heads: bfloat16 [32768, 512], P('sp'), may hold values from -4 to 4
- sink_logit: float32 [16], P('tp'), may hold values from -2 to 7
- out_weight: bfloat16 [2048, 2048], P('tp'), may hold values from -0.125 to 0.125
- residual: bfloat16 [32768, 2048], P(('sp', 'tp')), may hold values from -6 to 6
- mixer_gain: float32 [2048], replicated, may hold values from 0.1 to 1.9
- expert_gain: float32 [2048], replicated, may hold values from 0.1 to 1.9
- route_group: int32 [32768], P(('sp', 'tp')), may hold values from 0 to 15, as said below
- route_member: int32 [32768, 2], P(('sp', 'tp')), may hold values from 0 to 2, as said below
- route_weight: bfloat16 [32768, 2], P(('sp', 'tp')), may hold values from 0.19921875 to 1
- gate_weight: bfloat16 [48, 2048, 2048], P('sp', None, 'tp'), may hold values from -0.125 to 0.125
- up_weight: bfloat16 [48, 2048, 2048], P('sp', None, 'tp'), may hold values from -0.125 to 0.125
- down_weight: bfloat16 [48, 2048, 2048], P('sp', 'tp'), may hold values from -0.125 to 0.125
Outputs:
- output: bfloat16 [32768, 2048], P(('sp', 'tp'))
Inputs may be any that keep to these rules, and one draw needn't show every extreme that they name: `route_group`: among the tokens of one device, at most 10 name one group; in every draw one group is named by exactly 10 tokens of every device. `route_member`: the two entries of a token are different members of its group.
All inputs are finite; a program needn't handle non-finite values.
Results may differ from a plain program's by a relative error of at most 0.018.
Values may be sent and summed in bfloat16 or wider, within the bound.
A program may use at most 128 MiB of HBM per device.

v0:
```python
import jax
import jax.numpy as jnp
from jax import lax
from jax.sharding import Mesh
from jax.sharding import PartitionSpec as P

HEADS = 16
KV_HEADS = 4
HEAD_DIM = 128
WINDOW = 128
BLOCK = 128
GROUP_EXPERTS = 3
TP = ("tp_0", "tp_1")
SP_TP = ("sp", "tp_0", "tp_1")
EPS = 1e-06
NEG_BIG = -1e30


def extended(block, sides, width):
    for axis, dim in sides:
        count = lax.axis_size(axis)
        forward = [(i, i + 1) for i in range(count - 1)]
        backward = [(target, source) for source, target in forward]
        low = lax.ppermute(
            lax.slice_in_dim(block, block.shape[dim] - width, None, axis=dim), axis, forward
        )
        high = lax.ppermute(lax.slice_in_dim(block, 0, width, axis=dim), axis, backward)
        block = jnp.concatenate([low, block, high], axis=dim)
    return block


def cut_along(shard, dim, devices):
    dims = shard.shape
    blocks = shard.reshape(*dims[:dim], devices, dims[dim] // devices, *dims[dim + 1 :])
    return jnp.moveaxis(blocks, dim, 0)


def joined_along(blocks, dim):
    dims = list(blocks.shape[1:])
    dims[dim] *= blocks.shape[0]
    return jnp.moveaxis(blocks, 0, dim).reshape(dims)


def exchange_in_order(blocks, axes, order):
    dims = [lax.axis_size(a) for a in axes]
    blocks = blocks.reshape(*dims, *blocks.shape[1:])
    for k in order:
        blocks = lax.all_to_all(blocks, axes[k], split_axis=k, concat_axis=k, tiled=True)
    return blocks.reshape(-1, *blocks.shape[len(axes) :])


def stepwise_exchange(shard, axes, order, split_dim, concat_dim):
    blocks = cut_along(shard, split_dim, lax.axis_size(axes))
    return joined_along(exchange_in_order(blocks, axes, order), concat_dim)


def window_attention(queries, key_heads, value_heads, sink_logit):
    seq_rows = queries.shape[0]
    heads_dev = sink_logit.shape[0]
    key_group = HEADS // KV_HEADS
    key_start = lax.axis_index(TP) * heads_dev // key_group * HEAD_DIM
    key_own = lax.dynamic_slice_in_dim(key_heads, key_start, HEAD_DIM, 1)
    value_own = lax.dynamic_slice_in_dim(value_heads, key_start, HEAD_DIM, 1)
    padded = extended(jnp.stack([key_own, value_own]), (("sp", 1),), WINDOW)
    blocks = seq_rows // BLOCK
    extent = WINDOW // BLOCK
    tile_rows = padded.reshape(2, blocks + 2 * extent, BLOCK, HEAD_DIM)
    key_spans = jnp.concatenate(
        [tile_rows[:, shifted : shifted + blocks] for shifted in range(2 * extent + 1)], axis=2
    )
    offset = lax.axis_index("sp") * seq_rows
    seq_total = seq_rows * lax.axis_size("sp")
    query_pos = offset + jnp.arange(seq_rows, dtype=jnp.int32).reshape(blocks, BLOCK)
    key_pos = (
        offset
        + (jnp.arange(blocks, dtype=jnp.int32) * BLOCK)[:, None]
        + jnp.arange(BLOCK + 2 * WINDOW, dtype=jnp.int32)[None, :]
        - WINDOW
    )
    inside = (
        (jnp.abs(query_pos[:, :, None] - key_pos[:, None, :]) <= WINDOW)
        & (key_pos >= 0)[:, None, :]
        & (key_pos < seq_total)[:, None, :]
    )
    query_blocks = queries.reshape(blocks, BLOCK, heads_dev, HEAD_DIM)
    scores = jnp.einsum(
        "nqhd,nkd->nhqk", query_blocks, key_spans[0], preferred_element_type=jnp.float32
    ) * HEAD_DIM ** (-0.5)
    scores = jnp.where(inside[:, None], scores, NEG_BIG)
    sink_col = sink_logit[None, :, None, None]
    row_top = jnp.maximum(jnp.max(scores, axis=3, keepdims=True), sink_col)
    exp_terms = jnp.exp(scores - row_top)
    row_mass = jnp.sum(exp_terms, axis=3, keepdims=True) + jnp.exp(sink_col - row_top)
    weight = (exp_terms / row_mass).astype(jnp.bfloat16)
    attended = jnp.einsum(
        "nhqk,nkd->nqhd", weight, key_spans[1], preferred_element_type=jnp.float32
    ).astype(jnp.bfloat16)
    return attended.reshape(seq_rows, heads_dev * HEAD_DIM)


def per_device(
    queries,
    key_heads,
    value_heads,
    sink_logit,
    out_weight,
    residual,
    mixer_gain,
    expert_gain,
    route_group,
    route_member,
    route_weight,
    gate_weight,
    up_weight,
    down_weight,
):
    attended = window_attention(queries, key_heads, value_heads, sink_logit)
    tok_rows = residual.shape[0]
    width = out_weight.shape[1]
    by_token = stepwise_exchange(attended, TP, (1, 0), 0, 1)
    shard_rows = out_weight.shape[0]
    weight_piece = lax.all_gather(out_weight, TP, axis=0, tiled=True)
    shards = weight_piece.shape[0] // shard_rows
    columns = by_token
    columns = columns.reshape(tok_rows, shards, shard_rows)
    weight_slabs = weight_piece.reshape(shards, shard_rows, width)
    products = jnp.einsum("rkc,kcd->krd", columns, weight_slabs, preferred_element_type=jnp.float32)
    rounded = lax.optimization_barrier(products.astype(jnp.bfloat16))
    projected = jnp.sum(rounded.astype(jnp.float32), axis=0)
    proj_scale = lax.rsqrt(jnp.mean(projected * projected, axis=1, keepdims=True) + EPS)
    mixed_rows = (residual.astype(jnp.float32) + mixer_gain * (projected * proj_scale)).astype(
        jnp.bfloat16
    )
    mixed_float = mixed_rows.astype(jnp.float32)
    norm_scale = lax.rsqrt(jnp.mean(mixed_float * mixed_float, axis=1, keepdims=True) + EPS)
    normed = (mixed_float * norm_scale * expert_gain).astype(jnp.bfloat16)
    groups = lax.axis_size("sp")
    capacity = max(2, (5 * tok_rows + 4 * groups - 1) // (4 * groups))
    group_ids = jnp.arange(groups, dtype=jnp.int32)
    chosen = (route_group[:, None] == group_ids[None, :]).astype(jnp.int32)
    group_rank = jnp.sum(chosen * (jnp.cumsum(chosen, axis=0) - 1), axis=1)
    slot_ids = route_group * capacity + group_rank
    placing = (jnp.arange(groups * capacity, dtype=jnp.int32)[:, None] == slot_ids[None, :]).astype(
        jnp.bfloat16
    )
    member_ids = jnp.arange(GROUP_EXPERTS, dtype=jnp.int32)
    token_gates = jnp.sum(
        route_weight.astype(jnp.float32)[:, :, None]
        * (route_member[:, :, None] == member_ids[None, None, :]).astype(jnp.float32),
        axis=1,
    ).astype(jnp.bfloat16)
    send_rows = (
        jnp.dot(placing, normed, preferred_element_type=jnp.float32)
        .astype(jnp.bfloat16)
        .reshape(groups, capacity, width)
    )
    send_gates = (
        jnp.dot(placing, token_gates, preferred_element_type=jnp.float32)
        .astype(jnp.bfloat16)
        .reshape(groups, capacity, GROUP_EXPERTS)
    )
    arrived_rows, arrived_gates = (
        lax.all_to_all(send_rows, "sp", split_axis=0, concat_axis=0, tiled=True),
        lax.all_to_all(send_gates, "sp", split_axis=0, concat_axis=0, tiled=True),
    )
    pooled_rows, pooled_gates = (
        lax.all_gather(arrived_rows, TP, axis=0, tiled=True),
        lax.all_gather(arrived_gates, TP, axis=0, tiled=True),
    )
    flat_rows = pooled_rows.reshape(-1, width)
    flat_gates = pooled_gates.reshape(-1, GROUP_EXPERTS).astype(jnp.float32)
    gate_pre = jnp.einsum("md,edh->meh", flat_rows, gate_weight, preferred_element_type=jnp.float32)
    up_pre = jnp.einsum("md,edh->meh", flat_rows, up_weight, preferred_element_type=jnp.float32)
    hidden = (jax.nn.silu(gate_pre) * up_pre * flat_gates[:, :, None]).astype(jnp.bfloat16)
    partial_out = jnp.einsum("meh,ehd->md", hidden, down_weight, preferred_element_type=jnp.float32)
    summed = lax.psum_scatter(
        partial_out.reshape(pooled_rows.shape).astype(jnp.bfloat16),
        TP,
        scatter_dimension=0,
        tiled=True,
    )
    returned = lax.all_to_all(summed, "sp", split_axis=0, concat_axis=0, tiled=True)
    expert_out = lax.dot_general(
        placing,
        returned.reshape(groups * capacity, width),
        (((0,), (0,)), ((), ())),
        preferred_element_type=jnp.float32,
    )
    return (mixed_float + expert_out).astype(jnp.bfloat16)


def solution(mesh):
    torus = Mesh(mesh.devices.reshape(mesh.shape["sp"], 8, 2), ("sp", "tp_0", "tp_1"))
    placed = (
        P("sp", TP),
        P("sp", None),
        P("sp", None),
        P(TP),
        P(TP, None),
        P(SP_TP, None),
        P(),
        P(),
        P(SP_TP),
        P(SP_TP, None),
        P(SP_TP, None),
        P("sp", None, TP),
        P("sp", None, TP),
        P("sp", TP, None),
    )
    return jax.shard_map(
        per_device, mesh=torus, in_specs=placed, out_specs=P(SP_TP, None), check_vma=False
    )
```

profile of v0, /device:TPU:33, one launch (start us, length us, event | category | flops | bytes accessed | tf_op | source)
XLA Modules:
  0.0 387.4 jit_solution(15848808001674454527)
XLA Ops:
  6.5 0.7 all-gather.3.cloned.1.call-update
  7.3 1.3 dynamic-slice_bitcast_fusion
  8.6 3.1 collective-permute-start
  11.7 1.3 collective-permute-start.1
  13.7 0.1 fusion.22
  13.9 2.9 collective-permute-done.1
  16.7 0.1 pad_maximum_fusion.1
  16.8 0.8 fusion.25
  17.6 0.4 pad_maximum_fusion
  18.0 0.6 copy-done.6
  18.6 4.1 %fusion.26 = (f32[16,128]{1,0:T(8,128)S(1)}, f32[16,1,128,384]{2,3,0,1:T(8,128)S(1)}) fusion(bf16[16,128,128]{2,1,0:T(8,128)(2,1)S(1)} %bitcast.66, bf16[2,16,384,128]{3,2,1,0:T(8,128)(2,1)S(1)} %pad_maximum_fusion, pred[16,384]{1,0:T(8,128)(4,1)S(1)} %get-tuple-element.13, pred[16,384]{1,0:T(8,128)(4,1)S(1)} %get-tuple-element.12, ...), kind=kOutput, calls=%fused_computation.58 | convolution fusion | flops 207616000 | bytes 5296128 | tf_op jit(solution)/shard_map/nqhd,nkd->nhqk/dot_general | solution.py:86
  22.8 0.4 fusion.4
  23.2 1.0 fusion.8
  24.3 5.9 %all_to_all.25 = bf16[8,2,128,128]{2,3,0,1:T(8,128)(2,1)S(1)} all-to-all(bf16[8,2,128,128]{2,3,0,1:T(8,128)(2,1)S(1)} %copy.57), channel_id=1, replica_groups=mesh['sp'=16,'tp_0'=8,'tp_1'=2] {'tp_1'}, dimensions={1} | all-to-all | bytes 1048576 | tf_op jit(solution)/shard_map/all_to_all | solution.py:48
  30.2 0.8 copy.58
  31.1 8.0 %all-to-all-start.1 = ((bf16[8,2,128,128]{2,3,1,0:T(8,128)(2,1)}), bf16[8,2,128,128]{2,3,1,0:T(8,128)(2,1)S(1)}, u32[]{:S(2)}, u32[]{:S(2)}) async-start(bf16[8,2,128,128]{2,3,1,0:T(8,128)(2,1)} %copy.58), calls=%async_computation.1 | async-start | bytes 1048576 | tf_op jit(solution)/shard_map/all_to_all | solution.py:48
  39.1 0.1 fusion.17
  39.2 0.2 reduce_window_sum.11
  39.3 0.2 select_reduce_fusion
  39.5 21.6 %all-to-all-done.1 = bf16[8,2,128,128]{2,3,1,0:T(8,128)(2,1)S(1)} async-done(((bf16[8,2,128,128]{2,3,1,0:T(8,128)(2,1)}), bf16[8,2,128,128]{2,3,1,0:T(8,128)(2,1)S(1)}, u32[]{:S(2)}, u32[]{:S(2)}) %all-to-all-start.1) | async-done | bytes 524320 | tf_op jit(solution)/shard_map/all_to_all | solution.py:48
  61.1 0.3 copy.59
  61.4 16.1 %all-gather.3.cloned.1.call-done = bf16[2048,2048]{1,0:T(8,128)(2,1)} async-done(((bf16[128,2048]{1,0:T(8,128)(2,1)}), bf16[2048,2048]{1,0:T(8,128)(2,1)}) %all-gather.3.cloned.1.call-update) | async-done | bytes 8388624 | tf_op jit(solution)/shard_map/all_gather | solution.py:122
  77.5 5.7 %convolution_convert_fusion = bf16[16,128,2048]{2,1,0:T(8,128)(2,1)S(1)} fusion(bf16[128,16,128]{2,0,1:T(8,128)(2,1)S(1)} %bitcast.64, bf16[16,128,2048]{2,1,0:T(8,128)(2,1)} %bitcast.62), kind=kOutput, calls=%fused_computation.2 | convolution fusion | flops 1077936128 | bytes 17301504 | tf_op jit(solution)/shard_map/rkc,kcd->krd/dot_general | solution.py:127
  83.3 1.8 convert_reduce_fusion
  85.1 0.2 multiply_reduce_fusion
  85.3 0.4 fusion.11
  85.7 0.1 copy-done.3
  85.8 1.3 convolution_convert_fusion.1
  87.1 1.3 reshape.189
  88.4 22.7 %all_to_all.26 = bf16[16,10,2048]{2,1,0:T(8,128)(2,1)S(1)} all-to-all(bf16[16,10,2048]{2,1,0:T(8,128)(2,1)S(1)} %reshape.189), channel_id=1, replica_groups=mesh['sp'=16,'tp_0'=8,'tp_1'=2] {'sp'}, dimensions={0} | all-to-all | bytes 1310720 | tf_op jit(solution)/shard_map/all_to_all | solution.py:163
  111.1 1.2 copy.60
  112.5 0.1 convolution_convert_fusion.2
  112.6 0.1 reshape.191
  112.8 9.6 %all_to_all.27 = bf16[16,10,3]{1,2,0:T(4,128)(2,1)S(1)} all-to-all(bf16[16,10,3]{1,2,0:T(4,128)(2,1)S(1)} %copy.62), channel_id=1, replica_groups=mesh['sp'=16,'tp_0'=8,'tp_1'=2] {'sp'}, dimensions={0} | all-to-all | bytes 1920 | tf_op jit(solution)/shard_map/all_to_all | solution.py:164
  122.3 21.6 %all_gather.11 = bf16[256,10,3]{1,2,0:T(4,128)(2,1)S(1)} all-gather(bf16[16,10,3]{1,2,0:T(4,128)(2,1)S(1)} %all_to_all.27), channel_id=1, replica_groups=mesh['sp'=16,'tp_0'=8,'tp_1'=2] {'tp_0','tp_1'}, dimensions={0}, use_global_device_ids=true | all-gather | bytes 16320 | tf_op jit(solution)/shard_map/all_gather | solution.py:168
  144.0 0.2 copy.63
  144.1 0.2 copy.64
  144.3 0.3 reshape.193
  144.6 30.9 %all-gather.5.cloned.1.call-done = bf16[256,10,2048]{2,0,1:T(8,128)(2,1)} async-done(((bf16[16,10,2048]{2,0,1:T(8,128)(2,1)}), bf16[256,10,2048]{2,0,1:T(8,128)(2,1)}) %all-gather.5.cloned.1.call-update) | async-done | bytes 10485776 | tf_op jit(solution)/shard_map/all_gather | solution.py:167
  175.5 15.4 %copy.61 = bf16[256,10,2048]{2,1,0:T(8,128)(2,1)} copy(bf16[256,10,2048]{2,0,1:T(8,128)(2,1)} %all-gather.5.cloned.1.call-done) | data formatting | bytes 20971520 | tf_op jit(solution)/shard_map/all_gather | solution.py:167
  190.9 18.1 %reshape.194 = bf16[2560,2048,1]{1,0,2:T(8,128)(2,1)} reshape(bf16[256,10,2048]{2,1,0:T(8,128)(2,1)} %copy.61) | data formatting | bytes 20971520 | tf_op jit(solution)/shard_map/reshape | solution.py:170
  209.0 10.0 %fusion.27 = f32[2560,3,128]{2,0,1:T(8,128)} fusion(bf16[2560,2048,1]{1,0,2:T(8,128)(2,1)} %reshape.194, bf16[3,2048,128]{2,1,0:T(8,128)(2,1)} %param.25), kind=kOutput, calls=%fused_computation.59 | convolution fusion | flops 4026531840 | bytes 15990784 | tf_op jit(solution)/shard_map/md,edh->meh/dot_general | solution.py:172
  219.0 16.4 %bitcast_convert_fusion = bf16[2560,2048]{1,0:T(8,128)(2,1)} fusion(bf16[3,128,2048]{2,1,0:T(8,128)(2,1)S(1)} %copy-done, bf16[2560,2048,1]{1,0,2:T(8,128)(2,1)} %reshape.194, bf16[3,2048,128]{2,1,0:T(8,128)(2,1)} %param.26, f32[2560,3,128]{2,0,1:T(8,128)} %fusion.27, f32[2560,3]{0,1:T(4,128)S(1)} %reshape.193), kind=kOutput, calls=%fused_computation | convolution fusion | flops 8065187840 | bytes 28080128 | tf_op jit(solution)/shard_map/meh,ehd->md/dot_general | solution.py:175
  235.4 17.7 %convert_element_type.88 = bf16[256,10,2048]{2,1,0:T(8,128)(2,1)} reshape(bf16[2560,2048]{1,0:T(8,128)(2,1)} %bitcast_convert_fusion) | data formatting | bytes 20971520 | tf_op jit(solution)/shard_map/convert_element_type | solution.py:177
  253.1 99.7 %reduce-scatter.2.cloned.1.call-done = bf16[16,10,2048]{2,1,0:T(8,128)(2,1)} async-done(((bf16[256,10,2048]{2,1,0:T(8,128)(2,1)}), bf16[16,10,2048]{2,1,0:T(8,128)(2,1)}) %reduce-scatter.2.cloned.1.call-update) | async-done | bytes 655376 | tf_op jit(solution)/shard_map/reduce_scatter | solution.py:176
  352.8 24.8 %all_to_all.28 = bf16[16,10,2048]{2,1,0:T(8,128)(2,1)S(1)} all-to-all(bf16[16,10,2048]{2,1,0:T(8,128)(2,1)} %reduce-scatter.2.cloned.1.call-done), channel_id=1, replica_groups=mesh['sp'=16,'tp_0'=8,'tp_1'=2] {'sp'}, dimensions={0} | all-to-all | bytes 1310720 | tf_op jit(solution)/shard_map/all_to_all | solution.py:182
  377.6 1.1 reshape.192
  378.7 2.2 fusion.5
  (33 shorter events, 0.3 us)
Async XLA Ops:
  6.5 212.5 %copy-start = (bf16[3,128,2048]{2,1,0:T(8,128)(2,1)S(1)}, bf16[3,128,2048]{2,1,0:T(8,128)(2,1)}, u32[]{:S(2)}) copy-start(bf16[3,128,2048]{2,1,0:T(8,128)(2,1)} %param.27) | copy-start | bytes 4718596
  6.5 71.0 %all-gather.3.cloned.1.call-start = ((), (), s32[]{:S(2)}) async-start(), calls=%async_computation.6 | async-start | bytes 8912896 | tf_op jit(solution)/shard_map/all_gather | solution.py:122
  8.6 5.3 %collective-permute-start = (bf16[2,128,128]{2,1,0:T(8,128)(2,1)S(1)}, bf16[2,128,128]{2,1,0:T(8,128)(2,1)S(1)}, u32[]{:S(2)}, u32[]{:S(2)}) collective-permute-start(bf16[2,128,128]{2,1,0:T(8,128)(2,1)S(1)} %get-tuple-element.10), channel_id=1, source_target_pairs={{0,16},{16,32},{32,48},{48,64},{64,80},{80,96},{96,112},{112,128},... | collective-permute-start | bytes 196616 | tf_op jit(solution)/shard_map/ppermute | solution.py:24
  11.7 5.0 %collective-permute-start.1 = (bf16[2,128,128]{2,1,0:T(8,128)(2,1)S(1)}, bf16[2,128,128]{2,1,0:T(8,128)(2,1)S(1)}, u32[]{:S(2)}, u32[]{:S(2)}) collective-permute-start(bf16[2,128,128]{2,1,0:T(8,128)(2,1)S(1)} %get-tuple-element.11), channel_id=1, source_target_pairs={{16,0},{32,16},{48,32},{64,48},{80,64},{96,80},{112,96},{128,112},... | collective-permute-start | bytes 196616 | tf_op jit(solution)/shard_map/ppermute | solution.py:27
  17.6 1.0 copy-start.6
  24.3 14.8 %copy-start.4 = (s32[128]{0:T(128)S(1)}, s32[128]{0:T(128)}, u32[]{:S(2)}) copy-start(s32[128]{0:T(128)} %param.22) | copy-start | bytes 1540
  31.1 30.1 %all-to-all-start.1 = ((bf16[8,2,128,128]{2,3,1,0:T(8,128)(2,1)}), bf16[8,2,128,128]{2,3,1,0:T(8,128)(2,1)S(1)}, u32[]{:S(2)}, u32[]{:S(2)}) async-start(bf16[8,2,128,128]{2,3,1,0:T(8,128)(2,1)} %copy.58), calls=%async_computation.1 | async-start | bytes 1048576 | tf_op jit(solution)/shard_map/all_to_all | solution.py:48
  39.1 136.5 %all-gather.5.cloned.1.call-start = ((), (), s32[]{:S(2)}) async-start(), calls=%async_computation.7 | async-start | bytes 11141120 | tf_op jit(solution)/shard_map/all_gather | solution.py:167
  83.2 2.1 copy-start.1
  83.2 2.0 copy-start.2
  85.1 0.7 copy-start.3
  87.1 25.4 %copy-start.7 = (bf16[128,2]{0,1:T(2,128)(2,1)S(1)}, bf16[128,2]{0,1:T(2,128)(2,1)}, u32[]{:S(2)}) copy-start(bf16[128,2]{0,1:T(2,128)(2,1)} %param.24) | copy-start | bytes 1540
  87.1 25.4 %copy-start.5 = (s32[128,2]{0,1:T(2,128)S(1)}, s32[128,2]{0,1:T(2,128)}, u32[]{:S(2)}) copy-start(s32[128,2]{0,1:T(2,128)} %param.23) | copy-start | bytes 3076
  112.4 240.4 %reduce-scatter.2.cloned.1.call-start = ((), (), s32[]{:S(2)}) async-start(), calls=%async_computation.8 | async-start | bytes 17825792 | tf_op jit(solution)/shard_map/reduce_scatter | solution.py:176
Sparse Core Ops, SparseCore 0:
  9.2 68.3 all-gather.2
  112.5 62.9 all-gather.4
  253.2 99.5 reduce-scatter.1
where the time goes:
time: 389 us; the launch traced here: 387 us
  waiting for transfers between devices  172 us (44%)
  blocking collectives  84.6 us (22%)
  local copies, waits for them, and re-layouts  59.5 us (15%)
  matrix products  40.9 us (11%)
  between operations  14 us (4%)
  starting transfers between devices  12.5 us (3%)
  other arithmetic  3.92 us (1%)
    reduce_scatter x1, waiting for transfers between devices, per_device(): lax.psum_scatter(partial_out.reshape(pooled_rows.shape).astype(jnp.bfloat...  99.7 us
    all_gather x1, waiting for transfers between devices, per_device(): lax.all_gather(arrived_rows, TP, axis=0, tiled=True)  30.9 us
    all_to_all x1, blocking collectives, per_device(): lax.all_to_all(summed, 'sp', split_axis=0, concat_axis=0, tiled=True)  24.8 us
    all_to_all x1, blocking collectives, per_device(): lax.all_to_all(send_rows, 'sp', split_axis=0, concat_axis=0, tiled=True)  22.7 us
    all_gather x1, blocking collectives, per_device(): lax.all_gather(arrived_gates, TP, axis=0, tiled=True)  21.6 us
    all_to_all x1, waiting for transfers between devices, exchange_in_order(): lax.all_to_all(blocks, axes[k], split_axis=k, concat_axis=k, tiled=True)  21.6 us
    reshape x1, local copies, waits for them, and re-layouts, per_device(): flat_rows = pooled_rows.reshape(-1, width)  18.1 us
    convert_element_type x1, local copies, waits for them, and re-layouts, per_device(): partial_out.reshape(pooled_rows.shape).astype(jnp.bfloat16)  17.7 us
  transfers between devices with their start and end apart: 6, of which 5 were waited for; matrix products, arithmetic and copies ran while one was open for 3% of the time, Pallas kernels for 0%

commit v1 on v0

--- a/solution.py
+++ b/solution.py
@@ -14,6 +14,11 @@
 SP_TP = ("sp", "tp_0", "tp_1")
 EPS = 1e-06
 NEG_BIG = -1e30
+
+
+def all_by_exchange(value, axis, dim):
+    stack = jnp.stack([value] * lax.axis_size(axis))
+    return jnp.concatenate(lax.all_to_all(stack, axis, 0, 0), axis=dim)
 
 
 def extended(block, sides, width):
@@ -164,7 +169,7 @@
         lax.all_to_all(send_gates, "sp", split_axis=0, concat_axis=0, tiled=True),
     )
     pooled_rows, pooled_gates = (
-        lax.all_gather(arrived_rows, TP, axis=0, tiled=True),
+        all_by_exchange(arrived_rows, TP, 0),
         lax.all_gather(arrived_gates, TP, axis=0, tiled=True),
     )
     flat_rows = pooled_rows.reshape(-1, width)

time: 389 us -> 587 us (1.51)
  blocking collectives: 84.6 us -> 270 us
  starting transfers between devices: 12.5 us -> 32 us
  waiting for transfers between devices: 172 us -> 158 us
  local copies, waits for them, and re-layouts: 59.5 us -> 66.3 us
    all_gather x1, blocking collectives: 21.6 us -> 239 us  [per_device(): lax.all_gather(arrived_gates, TP, axis=0, tiled=True)]
    all_to_all x2 -> x0, blocking collectives: 32.3 us -> none  [the longest x1 22.7 us: per_device(): lax.all_to_all(send_rows, 'sp', split_axis=0, concat_axis=0, tiled=True)]
    all_gather x1 -> x0, waiting for transfers between devices: 30.9 us -> none  [per_device(): lax.all_gather(arrived_rows, TP, axis=0, tiled=True)]
    another operation x0 -> x2, local copies, waits for them, and re-layouts: none -> 24.5 us  [the longest x1 18.1 us: per_device(): flat_rows = pooled_rows.reshape(-1, width)]
    all_to_all x0 -> x3, waiting for transfers between devices: none -> 20.7 us  [the longest x1 15.5 us: per_device(): lax.all_to_all(send_rows, 'sp', split_axis=0, concat_axis=0, tiled=True)]
    all_to_all x0 -> x3, starting transfers between devices: none -> 19.6 us  [the longest x1 8.57 us: all_by_exchange(): return jnp.concatenate(lax.all_to_all(stack, axis, 0, 0), axis=dim)]
    reshape x1 -> x0, local copies, waits for them, and re-layouts: 18.1 us -> none  [per_device(): flat_rows = pooled_rows.reshape(-1, width)]
    all_gather x1 -> x0, local copies, waits for them, and re-layouts: 15.4 us -> none  [per_device(): lax.all_gather(arrived_rows, TP, axis=0, tiled=True)]
  transfers between devices with their start and end apart: 6 -> 8, of which waited for: 5 -> 6; matrix products, arithmetic and copies ran while one was open for 3% -> 2% of each run, Pallas kernels for 0% -> 0%
where the time goes in v1:
time: 587 us; the launch traced here: 585 us
  blocking collectives  270 us (46%)
  waiting for transfers between devices  158 us (27%)
  local copies, waits for them, and re-layouts  66.3 us (11%)
  matrix products  40 us (7%)
  starting transfers between devices  32 us (5%)
  between operations  14.4 us (2%)
    all_gather x1, blocking collectives, per_device(): lax.all_gather(arrived_gates, TP, axis=0, tiled=True)  239 us
    reduce_scatter x1, waiting for transfers between devices, per_device(): lax.psum_scatter(partial_out.reshape(pooled_rows.shape).astype(jnp.bfloat...  96.2 us
    all_to_all x1, blocking collectives, per_device(): lax.all_to_all(summed, 'sp', split_axis=0, concat_axis=0, tiled=True)  24.8 us
    all_to_all x1, waiting for transfers between devices, exchange_in_order(): lax.all_to_all(blocks, axes[k], split_axis=k, concat_axis=k, tiled=True)  21.6 us
    another operation x1, local copies, waits for them, and re-layouts, per_device(): flat_rows = pooled_rows.reshape(-1, width)  18.1 us
    convert_element_type x1, local copies, waits for them, and re-layouts, per_device(): partial_out.reshape(pooled_rows.shape).astype(jnp.bfloat16)  17.7 us
    dot_general x1, matrix products, per_device(): jnp.einsum('meh,ehd->md', hidden, down_weight, preferred_element_type=jnp...  16.4 us
    all_gather x1, waiting for transfers between devices, per_device(): weight_piece = lax.all_gather(out_weight, TP, axis=0, tiled=True)  16.1 us
  transfers between devices with their start and end apart: 8, of which 6 were waited for; matrix products, arithmetic and copies ran while one was open for 2% of the time, Pallas kernels for 0%

profile of v1, /device:TPU:33, one launch (start us, length us, event | category | flops | bytes accessed | tf_op | source)
XLA Modules:
  0.0 584.6 jit_solution(15012397416453293349)
XLA Ops:
  6.5 0.7 all-gather.2.cloned.1.call-update
  7.3 1.3 dynamic-slice_bitcast_fusion
  8.6 3.1 collective-permute-start
  11.7 1.3 collective-permute-start.1
  13.9 2.9 collective-permute-done.1
  16.8 0.8 fusion.25
  17.6 0.4 pad_maximum_fusion
  18.0 0.6 copy-done.6
  18.6 4.1 fusion.26
  22.8 0.4 fusion.4
  23.2 1.0 fusion.8
  24.3 5.9 %all_to_all.30 = bf16[8,2,128,128]{2,3,0,1:T(8,128)(2,1)S(1)} all-to-all(bf16[8,2,128,128]{2,3,0,1:T(8,128)(2,1)S(1)} %copy.57), channel_id=1, replica_groups=mesh['sp'=16,'tp_0'=8,'tp_1'=2] {'tp_1'}, dimensions={1} | all-to-all | bytes 1048576 | tf_op jit(solution)/shard_map/all_to_all | solution.py:53
  30.2 0.8 copy.58
  31.1 8.0 %all-to-all-start.1 = ((bf16[8,2,128,128]{2,3,1,0:T(8,128)(2,1)}), bf16[8,2,128,128]{2,3,1,0:T(8,128)(2,1)S(1)}, u32[]{:S(2)}, u32[]{:S(2)}) async-start(bf16[8,2,128,128]{2,3,1,0:T(8,128)(2,1)} %copy.58), calls=%async_computation.1 | async-start | bytes 1048576 | tf_op jit(solution)/shard_map/all_to_all | solution.py:53
  39.1 0.2 reduce_window_sum.11
  39.3 0.2 select_reduce_fusion
  39.5 21.6 %all-to-all-done.1 = bf16[8,2,128,128]{2,3,1,0:T(8,128)(2,1)S(1)} async-done(((bf16[8,2,128,128]{2,3,1,0:T(8,128)(2,1)}), bf16[8,2,128,128]{2,3,1,0:T(8,128)(2,1)S(1)}, u32[]{:S(2)}, u32[]{:S(2)}) %all-to-all-start.1) | async-done | bytes 524320 | tf_op jit(solution)/shard_map/all_to_all | solution.py:53
  61.1 0.3 copy.59
  61.4 16.1 %all-gather.2.cloned.1.call-done = bf16[2048,2048]{1,0:T(8,128)(2,1)} async-done(((bf16[128,2048]{1,0:T(8,128)(2,1)}), bf16[2048,2048]{1,0:T(8,128)(2,1)}) %all-gather.2.cloned.1.call-update) | async-done | bytes 8388624 | tf_op jit(solution)/shard_map/all_gather | solution.py:127
  77.5 5.7 convolution_convert_fusion
  83.3 1.8 convert_reduce_fusion
  85.1 0.2 multiply_reduce_fusion
  85.3 0.4 fusion.11
  85.8 0.4 convolution_convert_fusion.1
  86.2 1.2 reshape.188
  87.4 6.5 %all-to-all-start.2 = ((bf16[16,10,2048]{2,1,0:T(8,128)(2,1)}), bf16[16,10,2048]{2,1,0:T(8,128)(2,1)S(1)}, u32[]{:S(2)}, u32[]{:S(2)}) async-start(bf16[16,10,2048]{2,1,0:T(8,128)(2,1)} %reshape.188), calls=%async_computation.2 | async-start | bytes 2097152 | tf_op jit(solution)/shard_map/all_to_all | solution.py:168
  94.0 0.1 convolution_convert_fusion.2
  94.1 0.1 reshape.189
  94.2 0.6 copy.62
  94.8 15.5 %all-to-all-done.2 = bf16[16,10,2048]{2,1,0:T(8,128)(2,1)S(1)} async-done(((bf16[16,10,2048]{2,1,0:T(8,128)(2,1)}), bf16[16,10,2048]{2,1,0:T(8,128)(2,1)S(1)}, u32[]{:S(2)}, u32[]{:S(2)}) %all-to-all-start.2) | async-done | bytes 655392 | tf_op jit(solution)/shard_map/all_to_all | solution.py:168
  110.3 4.5 all-to-all-start.4
  114.9 1.2 copy.60
  116.1 5.2 all-to-all-done.4
  121.3 6.4 %stack.11 = bf16[16,16,10,2048]{3,1,2,0:T(8,128)(2,1)} broadcast(bf16[16,10,2048]{2,0,1:T(8,128)(2,1)} %copy.60), dimensions={1,2,3} | broadcast | bytes 11141120 | tf_op jit(solution)/shard_map/stack | solution.py:20
  127.7 8.6 %all-to-all-start.3 = ((bf16[16,16,10,2048]{3,1,2,0:T(8,128)(2,1)}), bf16[16,16,10,2048]{3,1,2,0:T(8,128)(2,1)}, u32[]{:S(2)}, u32[]{:S(2)}) async-start(bf16[16,16,10,2048]{3,1,2,0:T(8,128)(2,1)} %stack.11), calls=%async_computation.3 | async-start | bytes 20971520 | tf_op jit(solution)/shard_map/all_to_all | solution.py:21
  136.3 239.0 %all_gather.7 = bf16[256,10,3]{1,2,0:T(4,128)(2,1)S(1)} all-gather(bf16[16,10,3]{1,2,0:T(4,128)(2,1)S(1)} %all-to-all-done.4), channel_id=1, replica_groups=mesh['sp'=16,'tp_0'=8,'tp_1'=2] {'tp_0','tp_1'}, dimensions={0}, use_global_device_ids=true | all-gather | bytes 16320 | tf_op jit(solution)/shard_map/all_gather | solution.py:173
  375.3 0.2 copy.63
  375.5 0.2 copy.64
  375.7 0.3 reshape.191
  375.9 15.4 %copy.61 = bf16[16,16,10,2048]{3,2,1,0:T(8,128)(2,1)} copy(bf16[16,16,10,2048]{3,1,2,0:T(8,128)(2,1)} %all-to-all-done.3) | data formatting | bytes 20971520 | tf_op jit(solution)/shard_map/all_to_all | solution.py:21
  391.3 18.1 %reshape.192 = bf16[2560,2048,1]{1,0,2:T(8,128)(2,1)} reshape(bf16[16,16,10,2048]{3,2,1,0:T(8,128)(2,1)} %copy.61) | data formatting | bytes 20971520 | tf_op jit(solution)/shard_map/reshape;reshape | solution.py:175
  409.4 10.0 %fusion.27 = f32[2560,3,128]{2,0,1:T(8,128)} fusion(bf16[2560,2048,1]{1,0,2:T(8,128)(2,1)} %reshape.192, bf16[3,2048,128]{2,1,0:T(8,128)(2,1)} %param.25), kind=kOutput, calls=%fused_computation.59 | convolution fusion | flops 4026531840 | bytes 15990784 | tf_op jit(solution)/shard_map/md,edh->meh/dot_general | solution.py:177
  419.4 16.4 %bitcast_convert_fusion = bf16[2560,2048]{1,0:T(8,128)(2,1)} fusion(bf16[3,128,2048]{2,1,0:T(8,128)(2,1)S(1)} %copy-done, bf16[2560,2048,1]{1,0,2:T(8,128)(2,1)} %reshape.192, bf16[3,2048,128]{2,1,0:T(8,128)(2,1)} %param.26, f32[2560,3,128]{2,0,1:T(8,128)} %fusion.27, f32[2560,3]{0,1:T(4,128)S(1)} %reshape.191), kind=kOutput, calls=%fused_computation | convolution fusion | flops 8065187840 | bytes 28080128 | tf_op jit(solution)/shard_map/meh,ehd->md/dot_general | solution.py:180
  435.8 17.7 %convert_element_type.88 = bf16[256,10,2048]{2,1,0:T(8,128)(2,1)} reshape(bf16[2560,2048]{1,0:T(8,128)(2,1)} %bitcast_convert_fusion) | data formatting | bytes 20971520 | tf_op jit(solution)/shard_map/convert_element_type | solution.py:182
  453.5 96.2 %reduce-scatter.2.cloned.1.call-done = bf16[16,10,2048]{2,1,0:T(8,128)(2,1)} async-done(((bf16[256,10,2048]{2,1,0:T(8,128)(2,1)}), bf16[16,10,2048]{2,1,0:T(8,128)(2,1)}) %reduce-scatter.2.cloned.1.call-update) | async-done | bytes 655376 | tf_op jit(solution)/shard_map/reduce_scatter | solution.py:181
  549.7 24.8 %all_to_all.31 = bf16[16,10,2048]{2,1,0:T(8,128)(2,1)S(1)} all-to-all(bf16[16,10,2048]{2,1,0:T(8,128)(2,1)} %reduce-scatter.2.cloned.1.call-done), channel_id=1, replica_groups=mesh['sp'=16,'tp_0'=8,'tp_1'=2] {'sp'}, dimensions={0} | all-to-all | bytes 1310720 | tf_op jit(solution)/shard_map/all_to_all | solution.py:187
  574.5 1.1 reshape.190
  575.5 2.2 fusion.5
  (35 shorter events, 0.6 us)
Async XLA Ops:
  6.5 412.8 %copy-start = (bf16[3,128,2048]{2,1,0:T(8,128)(2,1)S(1)}, bf16[3,128,2048]{2,1,0:T(8,128)(2,1)}, u32[]{:S(2)}) copy-start(bf16[3,128,2048]{2,1,0:T(8,128)(2,1)} %param.27) | copy-start | bytes 4718596
  6.5 71.0 %all-gather.2.cloned.1.call-start = ((), (), s32[]{:S(2)}) async-start(), calls=%async_computation.7 | async-start | bytes 8912896 | tf_op jit(solution)/shard_map/all_gather | solution.py:127
  8.6 5.3 collective-permute-start
  11.7 5.0 collective-permute-start.1
  17.6 1.0 copy-start.6
  24.3 14.8 %copy-start.4 = (s32[128]{0:T(128)S(1)}, s32[128]{0:T(128)}, u32[]{:S(2)}) copy-start(s32[128]{0:T(128)} %param.22) | copy-start | bytes 1540
  31.1 30.1 %all-to-all-start.1 = ((bf16[8,2,128,128]{2,3,1,0:T(8,128)(2,1)}), bf16[8,2,128,128]{2,3,1,0:T(8,128)(2,1)S(1)}, u32[]{:S(2)}, u32[]{:S(2)}) async-start(bf16[8,2,128,128]{2,3,1,0:T(8,128)(2,1)} %copy.58), calls=%async_computation.1 | async-start | bytes 1048576 | tf_op jit(solution)/shard_map/all_to_all | solution.py:53
  83.2 2.1 copy-start.1
  83.2 2.0 copy-start.2
  85.1 0.7 copy-start.3
  85.3 8.6 %copy-start.7 = (bf16[128,2]{0,1:T(2,128)(2,1)S(1)}, bf16[128,2]{0,1:T(2,128)(2,1)}, u32[]{:S(2)}) copy-start(bf16[128,2]{0,1:T(2,128)(2,1)} %param.24) | copy-start | bytes 1540
  85.3 8.6 %copy-start.5 = (s32[128,2]{0,1:T(2,128)S(1)}, s32[128,2]{0,1:T(2,128)}, u32[]{:S(2)}) copy-start(s32[128,2]{0,1:T(2,128)} %param.23) | copy-start | bytes 3076
  87.4 22.9 %all-to-all-start.2 = ((bf16[16,10,2048]{2,1,0:T(8,128)(2,1)}), bf16[16,10,2048]{2,1,0:T(8,128)(2,1)S(1)}, u32[]{:S(2)}, u32[]{:S(2)}) async-start(bf16[16,10,2048]{2,1,0:T(8,128)(2,1)} %reshape.188), calls=%async_computation.2 | async-start | bytes 2097152 | tf_op jit(solution)/shard_map/all_to_all | solution.py:168
  110.3 10.9 %all-to-all-start.4 = ((bf16[16,10,3]{1,2,0:T(4,128)(2,1)}), bf16[16,10,3]{1,2,0:T(4,128)(2,1)S(1)}, u32[]{:S(2)}, u32[]{:S(2)}) async-start(bf16[16,10,3]{1,2,0:T(4,128)(2,1)} %copy.62), calls=%async_computation.4 | async-start | bytes 32768 | tf_op jit(solution)/shard_map/all_to_all | solution.py:169
  127.7 248.2 %all-to-all-start.3 = ((bf16[16,16,10,2048]{3,1,2,0:T(8,128)(2,1)}), bf16[16,16,10,2048]{3,1,2,0:T(8,128)(2,1)}, u32[]{:S(2)}, u32[]{:S(2)}) async-start(bf16[16,16,10,2048]{3,1,2,0:T(8,128)(2,1)} %stack.11), calls=%async_computation.3 | async-start | bytes 20971520 | tf_op jit(solution)/shard_map/all_to_all | solution.py:21
  136.3 413.4 %reduce-scatter.2.cloned.1.call-start = ((), (), s32[]{:S(2)}) async-start(), calls=%async_computation.8 | async-start | bytes 17825792 | tf_op jit(solution)/shard_map/reduce_scatter | solution.py:181
Sparse Core Ops, SparseCore 0:
  9.2 68.3 all-gather.1
  453.6 96.0 reduce-scatter.1
